TPU v7x, 512 devices: a whole 4x8x8 slice. The times are simulated.
512 devices in a mesh: fs: 64 (over z, y), rep: 4 (over x), tp: 2 (over core).
Axes of the slice: x: 4, y: 8, z: 8, core: 2. Of those that a mesh axis runs over, the one named last changes fastest.
Arguments:
- saved_in: bfloat16 [65536, 4096], P(('fs', 'rep', 'tp')), may hold values from -6 to 6
- out_cot: bfloat16 [65536, 4096], P(('fs', 'rep', 'tp')), may hold values from -0.0234375 to 0.0234375
- value_cot: bfloat16 [65536, 2048], P(('fs', 'rep'), 'tp'), may hold values from -0.0234375 to 0.0234375
- mixed_out: bfloat16 [65536, 2048], P(('fs', 'rep'), 'tp'), may hold values from -6 to 6
- value_factor: bfloat16 [4096, 512], P('fs'), may hold values from -0.09375 to 0.09375
- out_factor: bfloat16 [4096, 512], P('fs'), may hold values from -0.09375 to 0.09375
- value_weight: float32 [4096, 2048], P('fs', 'tp'), may hold values from -0.09375 to 0.09375
- out_weight: float32 [2048, 4096], P('tp', 'fs'), may hold values from -0.125 to 0.125
- value_first: float32 [512, 2048], P('fs', 'tp'), may hold values from -6 to 6
- value_second: float32 [512, 2048], P('fs', 'tp'), may hold values from 0.25 to 4
- out_first: float32 [512, 2048], P('fs', 'tp'), may hold values from -6 to 6
- out_second: float32 [512, 2048], P('fs', 'tp'), may hold values from 0.25 to 4
Outputs:
- value_weight_new: float32 [4096, 2048], P('fs', 'tp')
- value_weight_copy: bfloat16 [4096, 2048], P('fs', 'tp')
- out_weight_new: float32 [2048, 4096], P('tp', 'fs')
- out_weight_copy: bfloat16 [2048, 4096], P('tp', 'fs')
- value_first_new: float32 [512, 2048], P('fs', 'tp')
- value_second_new: float32 [512, 2048], P('fs', 'tp')
- out_first_new: float32 [512, 2048], P('fs', 'tp')
- out_second_new: float32 [512, 2048], P('fs', 'tp')
- value_step: float32 [512, 2048], P('fs', 'tp')
- out_step: float32 [512, 2048], P('fs', 'tp')
All inputs are finite; a program needn't handle non-finite values.
Results may differ from a plain program's by a relative error of at most 0.005.
Values may be sent and summed in bfloat16 or wider, within the bound.
A program may use at most 64 MiB of HBM per device.

v0:
```python
import functools

import jax
import jax.numpy as jnp
from jax import lax
from jax.sharding import Mesh
from jax.sharding import PartitionSpec as P

CHANNELS = 2048
RANK = 512
FS = ("fs_0", "fs_1")
FS_TP = ("fs_0", "fs_1", "tp")
FS_REP_TP = ("fs_0", "fs_1", "rep", "tp")
FS_REP = ("fs_0", "fs_1", "rep")


beta_first = 0.8
beta_second = 0.9
step_rate = 0.05
clip_level = 0.5


def sent_together(arrays, axis, dim, along):
    both = jnp.concatenate(arrays, axis=along)
    result, at, outs = (lax.all_gather(both, axis, axis=dim, tiled=True), 0, [])
    for a in arrays:
        outs.append(lax.slice_in_dim(result, at, at + a.shape[along], axis=along))
        at += a.shape[along]
    return tuple(outs)


def own_rows(so_far, axes):
    for axis in axes:
        so_far = lax.psum_scatter(so_far, axis, scatter_dimension=0, tiled=True)
    return so_far


def from_everyone(array, axis):
    peers = lax.axis_size(axis)
    return lax.all_to_all(
        jnp.broadcast_to(array[None], (peers, *array.shape)), axis, 0, 0, tiled=True
    )


def of_everyone(array, axis):
    return from_everyone(array, axis).astype(jnp.float32).sum(axis=0)


def in_order(blocks, dim):
    shape = list(blocks.shape[1:])
    shape[dim] *= blocks.shape[0]
    return jnp.moveaxis(blocks, 0, dim).reshape(shape)


def stacked_from(array, axes, turns):
    blocks = array
    for k in turns:
        blocks = lax.all_gather(blocks, axes[k])
    done = turns[::-1]
    back = [done.index(k) for k in range(len(axes))]
    blocks = blocks.transpose(*back, *range(len(axes), blocks.ndim))
    return blocks.reshape(-1, *array.shape)


def whole_of(array, axes, turns, dim):
    return in_order(stacked_from(array, axes, turns), dim)


def over_axes(array, axes):
    return functools.reduce(lax.psum, axes, array)


def fold_pair(left_in, left_cot, pieces):
    return (
        jnp.dot(left_in, pieces[0], preferred_element_type=jnp.float32),
        jnp.dot(left_cot, pieces[1], preferred_element_type=jnp.float32),
    )


def contract_rows(left, right):
    return lax.dot_general(
        left, right, (((0,), (0,)), ((), ())), preferred_element_type=jnp.float32
    )


def adapt(grad, first, second):
    new_first = beta_first * first + (1.0 - beta_first) * grad
    new_second = beta_second * second + (1.0 - beta_second) * grad * grad
    lowered = (new_first / jnp.sqrt(new_second)).astype(jnp.bfloat16)
    return (new_first, new_second, lowered)


def shards(
    saved_in,
    out_cot,
    value_cot,
    mixed_out,
    value_factor,
    out_factor,
    value_weight,
    out_weight,
    value_first,
    value_second,
    out_first,
    out_second,
):
    proj_in, proj_cot = fold_pair(
        saved_in, out_cot, sent_together((value_factor, out_factor), FS, 0, 1)
    )
    proj_in, proj_cot = sent_together(
        (proj_in.astype(jnp.bfloat16), proj_cot.astype(jnp.bfloat16)), "tp", 0, 1
    )
    summed = own_rows(
        jnp.concatenate(
            [contract_rows(proj_in, value_cot), contract_rows(proj_cot, mixed_out)], axis=1
        ),
        FS,
    )
    summed = of_everyone(summed.astype(jnp.bfloat16), "rep").astype(jnp.float32)
    chan_cols = value_cot.shape[1]
    value_first_new, value_second_new, low_value = adapt(
        summed[:, :chan_cols], value_first, value_second
    )
    out_first_new, out_second_new, low_out = adapt(summed[:, chan_cols:], out_first, out_second)
    lowered = jnp.concatenate([low_value, low_out], axis=1)
    gathered = whole_of(lowered, FS, (0, 1), 0)
    own_float = lowered.astype(jnp.float32)
    total = over_axes(jnp.sum(own_float * own_float), FS_TP)
    spread = jnp.sqrt(total / (2.0 * RANK * CHANNELS))
    scale = clip_level / jnp.maximum(spread, clip_level)
    value_full = jnp.dot(value_factor, gathered[:, :chan_cols], preferred_element_type=jnp.float32)
    out_full = lax.dot_general(
        gathered[:, chan_cols:],
        out_factor,
        (((0,), (1,)), ((), ())),
        preferred_element_type=jnp.float32,
    )
    value_weight_new = value_weight - step_rate * scale * value_full
    out_weight_new = out_weight - step_rate * scale * out_full
    return (
        value_weight_new,
        value_weight_new.astype(jnp.bfloat16),
        out_weight_new,
        out_weight_new.astype(jnp.bfloat16),
        value_first_new,
        value_second_new,
        out_first_new,
        out_second_new,
        scale * low_value.astype(jnp.float32),
        scale * low_out.astype(jnp.float32),
    )


def solution(mesh):
    torus = Mesh(
        mesh.devices.reshape(8, 8, mesh.shape["rep"], mesh.shape["tp"]),
        ("fs_0", "fs_1", "rep", "tp"),
    )
    placed = (
        P(FS_REP_TP, None),
        P(FS_REP_TP, None),
        P(FS_REP, "tp"),
        P(FS_REP, "tp"),
        P(FS, None),
        P(FS, None),
        P(FS, "tp"),
        P("tp", FS),
        P(FS, "tp"),
        P(FS, "tp"),
        P(FS, "tp"),
        P(FS, "tp"),
    )
    return jax.shard_map(
        shards,
        mesh=torus,
        in_specs=placed,
        out_specs=(
            P(FS, "tp"),
            P(FS, "tp"),
            P("tp", FS),
            P("tp", FS),
            P(FS, "tp"),
            P(FS, "tp"),
            P(FS, "tp"),
            P(FS, "tp"),
            P(FS, "tp"),
            P(FS, "tp"),
        ),
        check_vma=False,
    )
```

profile of v0, /device:TPU:1, one launch (start us, length us, event | category | flops | bytes accessed | tf_op | source)
XLA Modules:
  0.0 316.0 jit_solution(3303858645815986479)
XLA Ops:
  7.2 0.0 copy-start
  7.2 0.0 copy-start.11
  7.2 0.0 all-gather.5.cloned.1.call-start
  7.2 1.7 pad_maximum_fusion.2
  8.9 0.0 all-gather.5.cloned.1.call-update
  8.9 0.0 reduce-scatter.3.cloned.1.call-start
  9.0 107.0 %all-gather.5.cloned.1.call-done = bf16[4096,1024]{1,0:T(8,128)(2,1)} async-done(((bf16[64,1024]{1,0:T(8,128)(2,1)}), bf16[4096,1024]{1,0:T(8,128)(2,1)}) %all-gather.5.cloned.1.call-update) | async-done | bytes 8388624 | tf_op jit(solution)/shard_map/all_gather | solution.py:25
  116.0 0.0 copy-done
  116.0 3.5 %fusion.13 = bf16[128,512]{0,1:T(8,128)(2,1)S(1)} fusion(bf16[128,4096]{1,0:T(8,128)(2,1)S(1)} %copy-done, bf16[4096,1024]{1,0:T(8,128)(2,1)} %all-gather.5.cloned.1.call-done), kind=kOutput, calls=%fused_computation.12 | convolution fusion | flops 536936448 | bytes 5373952 | tf_op jit(solution)/shard_map/dot_general | solution.py:76
  119.5 0.0 copy-done.11
  119.5 0.0 copy-start.1
  119.5 0.0 copy-start.2
  119.5 3.6 %fusion.16 = bf16[128,512]{0,1:T(8,128)(2,1)S(1)} fusion(bf16[128,4096]{1,0:T(8,128)(2,1)S(1)} %copy-done.11, bf16[4096,1024]{1,0:T(8,128)(2,1)} %all-gather.5.cloned.1.call-done), kind=kOutput, calls=%fused_computation.13 | convolution fusion | flops 536936448 | bytes 5373952 | tf_op jit(solution)/shard_map/dot_general | solution.py:75
  123.1 2.8 all_gather.19
  125.9 0.0 copy-done.1
  125.9 0.4 fusion.21
  126.3 0.0 copy-done.2
  126.3 0.4 fusion.23
  126.8 2.4 pad_maximum_fusion
  129.2 0.0 copy-start.7
  129.2 0.0 copy-start.8
  129.2 0.0 copy-start.9
  129.2 0.0 copy-start.10
  129.2 0.0 reduce-scatter.3.cloned.1.call-update
  129.3 0.0 copy-start.3
  129.3 0.0 copy-start.5
  129.3 0.0 copy-start.4
  129.3 0.0 copy-start.6
  129.3 0.0 reduce-scatter.5.cloned.1.call-start
  129.4 56.5 %reduce-scatter.3.cloned.1.call-done = f32[64,2048]{1,0:T(8,128)} async-done(((f32[512,2048]{1,0:T(8,128)}), f32[64,2048]{1,0:T(8,128)}) %reduce-scatter.3.cloned.1.call-update) | async-done | bytes 524304 | tf_op jit(solution)/shard_map/reduce_scatter | solution.py:34
  185.8 0.0 reduce-scatter.5.cloned.1.call-update
  185.8 0.0 all-gather.7.cloned.1.call-start
  185.9 36.2 %reduce-scatter.5.cloned.1.call-done = f32[8,2048]{1,0:T(8,128)} async-done(((f32[64,2048]{1,0:T(8,128)}), f32[8,2048]{1,0:T(8,128)}) %reduce-scatter.5.cloned.1.call-update) | async-done | bytes 65552 | tf_op jit(solution)/shard_map/reduce_scatter | solution.py:34
  222.1 0.8 convert_element_type.43
  223.0 8.5 %all_to_all.5 = bf16[4,8,2048]{2,1,0:T(8,128)(2,1)S(1)} all-to-all(bf16[4,8,2048]{2,1,0:T(8,128)(2,1)S(1)} %broadcast_in_dim.2), channel_id=1, replica_groups=mesh['fs_0'=8,'fs_1'=8,'rep'=4,'tp'=2] {'rep'}, dimensions={0} | all-to-all | bytes 262144 | tf_op jit(solution)/shard_map/all_to_all | solution.py:40
  231.5 0.0 copy-done.7
  231.5 0.0 copy-done.8
  231.6 0.0 copy-done.9
  231.6 0.0 copy-done.10
  231.6 0.7 multiply_convert_fusion.1
  232.2 22.6 %all-gather = bf16[64,2048]{1,0:T(8,128)(2,1)} all-gather(bf16[8,2048]{1,0:T(8,128)(2,1)S(1)} %pad_maximum_fusion.3), channel_id=2, replica_groups=mesh['fs_0'=8,'fs_1'=8,'rep'=4,'tp'=2] {'fs_0'}, dimensions={0}, use_global_device_ids=true | all-gather | bytes 294912 | tf_op jit(solution)/shard_map/all_gather | solution.py:58
  254.9 0.0 all-gather.7.cloned.1.call-update
  254.9 0.6 multiply_reduce_fusion
  255.5 12.9 %psum.21 = f32[]{:T(128)} all-reduce(f32[]{:T(128)} %multiply_reduce_fusion), channel_id=1, replica_groups=mesh['fs_0'=8,'fs_1'=8,'rep'=4,'tp'=2] {'fs_0'}, use_global_device_ids=true, to_apply=%region_4.0 | all-reduce | flops 1 | bytes 8 | tf_op jit(solution)/shard_map/psum | solution.py:70
  268.5 13.0 %psum.22 = f32[]{:T(128)} all-reduce(f32[]{:T(128)} %psum.21), channel_id=1, replica_groups=mesh['fs_0'=8,'fs_1'=8,'rep'=4,'tp'=2] {'fs_1'}, use_global_device_ids=true, to_apply=%region_5.0 | all-reduce | flops 1 | bytes 8 | tf_op jit(solution)/shard_map/psum | solution.py:70
  281.5 22.7 %psum.23 = f32[]{:T(128)} all-reduce(f32[]{:T(128)} %psum.22), channel_id=1, replica_groups=mesh['fs_0'=8,'fs_1'=8,'rep'=4,'tp'=2] {'tp'}, use_global_device_ids=true, to_apply=%region_6.0 | all-reduce | flops 1 | bytes 8 | tf_op jit(solution)/shard_map/psum | solution.py:70
  305.0 0.6 convert_multiply_fusion
  305.6 0.0 all-gather.7.cloned.1.call-done
  305.6 1.7 copy.24
  307.3 0.0 copy-done.3
  307.3 0.0 copy-done.5
  307.3 1.0 fusion.30
  308.4 0.0 copy-done.4
  308.4 0.0 copy-done.6
  308.4 1.0 fusion.29
  (4 shorter events, 0.1 us)
Async XLA Ops:
  7.2 108.8 %copy-start = (bf16[128,4096]{1,0:T(8,128)(2,1)S(1)}, bf16[128,4096]{1,0:T(8,128)(2,1)}, u32[]{:S(2)}) copy-start(bf16[128,4096]{1,0:T(8,128)(2,1)} %param.13) | copy-start | bytes 3145732
  7.2 112.3 %copy-start.11 = (bf16[128,4096]{1,0:T(8,128)(2,1)S(1)}, bf16[128,4096]{1,0:T(8,128)(2,1)}, u32[]{:S(2)}) copy-start(bf16[128,4096]{1,0:T(8,128)(2,1)} %param.12) | copy-start | bytes 3145732
  7.2 108.8 %all-gather.5.cloned.1.call-start = ((), (), s32[]{:S(2)}) async-start(), calls=%async_computation.3 | async-start | bytes 8519680 | tf_op jit(solution)/shard_map/all_gather | solution.py:25
  8.9 176.9 %reduce-scatter.3.cloned.1.call-start = ((), (), s32[]{:S(2)}) async-start(), calls=%async_computation.4 | async-start | bytes 4718592 | tf_op jit(solution)/shard_map/reduce_scatter | solution.py:34
  119.5 6.4 %copy-start.1 = (bf16[256,1024]{1,0:T(8,128)(2,1)S(1)}, bf16[256,1024]{1,0:T(8,128)(2,1)}, u32[]{:S(2)}) copy-start(bf16[256,1024]{1,0:T(8,128)(2,1)} %param.15) | copy-start | bytes 1572868
  119.5 6.8 %copy-start.2 = (bf16[256,1024]{1,0:T(8,128)(2,1)S(1)}, bf16[256,1024]{1,0:T(8,128)(2,1)}, u32[]{:S(2)}) copy-start(bf16[256,1024]{1,0:T(8,128)(2,1)} %param.14) | copy-start | bytes 1572868
  129.2 102.3 %copy-start.7 = (f32[8,1024]{1,0:T(8,128)S(1)}, f32[8,1024]{1,0:T(8,128)}, u32[]{:S(2)}) copy-start(f32[8,1024]{1,0:T(8,128)} %param.21) | copy-start | bytes 98308
  129.2 102.3 %copy-start.8 = (f32[8,1024]{1,0:T(8,128)S(1)}, f32[8,1024]{1,0:T(8,128)}, u32[]{:S(2)}) copy-start(f32[8,1024]{1,0:T(8,128)} %param.20) | copy-start | bytes 98308
  129.2 102.3 %copy-start.9 = (f32[8,1024]{1,0:T(8,128)S(1)}, f32[8,1024]{1,0:T(8,128)}, u32[]{:S(2)}) copy-start(f32[8,1024]{1,0:T(8,128)} %param.23) | copy-start | bytes 98308
  129.2 102.3 %copy-start.10 = (f32[8,1024]{1,0:T(8,128)S(1)}, f32[8,1024]{1,0:T(8,128)}, u32[]{:S(2)}) copy-start(f32[8,1024]{1,0:T(8,128)} %param.22) | copy-start | bytes 98308
  129.3 178.1 %copy-start.3 = (f32[1024,64]{0,1:T(8,128)S(1)}, f32[1024,64]{0,1:T(8,128)}, u32[]{:S(2)}) copy-start(f32[1024,64]{0,1:T(8,128)} %param.19) | copy-start | bytes 786436
  129.3 178.1 %copy-start.5 = (bf16[64,512]{1,0:T(8,128)(2,1)S(1)}, bf16[64,512]{1,0:T(8,128)(2,1)}, u32[]{:S(2)}) copy-start(bf16[64,512]{1,0:T(8,128)(2,1)} %param.17) | copy-start | bytes 196612
  129.3 179.1 %copy-start.4 = (f32[64,1024]{1,0:T(8,128)S(1)}, f32[64,1024]{1,0:T(8,128)}, u32[]{:S(2)}) copy-start(f32[64,1024]{1,0:T(8,128)} %param.18) | copy-start | bytes 786436
  129.3 179.1 %copy-start.6 = (bf16[64,512]{1,0:T(8,128)(2,1)S(1)}, bf16[64,512]{1,0:T(8,128)(2,1)}, u32[]{:S(2)}) copy-start(bf16[64,512]{1,0:T(8,128)(2,1)} %param.16) | copy-start | bytes 196612
  129.3 92.8 %reduce-scatter.5.cloned.1.call-start = ((), (), s32[]{:S(2)}) async-start(), calls=%async_computation.5 | async-start | bytes 589824 | tf_op jit(solution)/shard_map/reduce_scatter | solution.py:34
  185.8 119.7 %all-gather.7.cloned.1.call-start = ((), (), s32[]{:S(2)}) async-start(), calls=%async_computation.6 | async-start | bytes 2359296 | tf_op jit(solution)/shard_map/all_gather | solution.py:58
Sparse Core Ops, SparseCore 0:
  11.6 104.3 all-gather.4
  129.4 56.3 reduce-scatter.2
  188.6 33.4 reduce-scatter.4
  255.0 46.8 all-gather.6
where the time goes:
time: 316 us
  waiting for transfers between devices  200 us (63%)
  blocking collectives  82.6 us (26%)
  between operations  14.7 us (5%)
  matrix products  10 us (3%)
  other arithmetic  6.91 us (2%)
    all_gather x1, waiting for transfers between devices, sent_together(): result, at, outs = (lax.all_gather(both, axis, axis=dim, tiled=True), 0, [])  107 us
    reduce_scatter x2, waiting for transfers between devices, own_rows(): so_far = lax.psum_scatter(so_far, axis, scatter_dimension=0, tiled=True)  92.7 us
    psum x3, blocking collectives, over_axes(): return functools.reduce(lax.psum, axes, array)  48.7 us
    all_gather x1, blocking collectives, stacked_from(): blocks = lax.all_gather(blocks, axes[k])  22.6 us
    all_to_all x1, blocking collectives, from_everyone(): lax.all_to_all(jnp.broadcast_to(array[None], (peers, *array.shape)), axis...  8.54 us
  transfers between devices with their start and end apart: 4, of which 3 were waited for; matrix products, arithmetic and copies ran while one was open for 0% of the time, Pallas kernels for 0%

commit v1 on v0

v1 whole, which is shorter than its diff:
```python
import jax
import jax.numpy as jnp
from jax import lax
from jax.experimental import pallas as pl
from jax.experimental.pallas import tpu as pltpu
from jax.sharding import Mesh
from jax.sharding import PartitionSpec as P

MESH = pl.DeviceIdType.MESH
FS = ("fs_0", "fs_1")
FS_REP_TP = ("fs_0", "fs_1", "rep", "tp")
FS_REP = ("fs_0", "fs_1", "rep")

beta_first = 0.8
beta_second = 0.9
step_rate = 0.05
clip_level = 0.5

SUBS = 2


def body(
    sizes,
    total_count,
    saved_in,
    out_cot,
    value_cot,
    mixed_out,
    value_factor,
    out_factor,
    value_weight,
    out_weight_t,
    value_first,
    value_second,
    out_first,
    out_second,
    vw_new,
    vw_copy,
    ow_new,
    ow_copy,
    vf_new,
    vs_new,
    of_new,
    os_new,
    v_step,
    o_step,
    factor,
    tokens,
    acc,
    cots,
    proj,
    grads,
    own_factor,
    weights,
    moments,
    send_1,
    recv_1,
    send_2,
    own_2,
    recv_2,
    recv_3,
    low,
    rows_low,
    product,
    squares,
    local_sem,
    tok_sem,
    ga_send,
    ga_recv,
    proj_sem,
    s1_send,
    s1_recv,
    s2_send,
    s2_recv,
    s3_send,
    s3_recv,
    e1_send,
    e1_recv,
    e2_send,
    e2_recv,
    xp_send,
    xp_recv,
    ss_send,
    ss_recv,
):
    nz, ny, nx = sizes
    z, y = lax.axis_index("fs_0"), lax.axis_index("fs_1")
    x, c = lax.axis_index("rep"), lax.axis_index("tp")
    shard = value_factor.shape[0]
    half = shard // 2
    mine = saved_in.shape[0]
    chans = value_cot.shape[1]
    quarter = chans // nx

    def at_z(d):
        return (lax.rem(z + d + nz, nz), y, x, c)

    def at_y(d):
        return (z, lax.rem(y + d + ny, ny), x, c)

    def at_x(d, core=0):
        return (z, y, lax.rem(x + d, nx), lax.rem(c + core, 2))

    pair = (z, y, x, 1 - c)

    peers = [at_z(d) for d in range(1, nz)] + [at_y(d) for d in range(1, ny)]
    peers += [at_x(d, k) for k in range(2) for d in range(nx) if (d, k) != (0, 0)]
    barrier = pltpu.get_barrier_semaphore()
    for peer in peers:
        pl.semaphore_signal(barrier, inc=1, device_id=peer, device_id_type=MESH)

    def local(src, dst, k):
        return pltpu.make_async_copy(src, dst, local_sem.at[k])

    def shard_rows(zi, yi, h):
        return pl.ds(pl.multiple_of((zi * ny + yi) * shard + h * half, half), half)

    own_rows = pl.ds(pl.multiple_of((z * ny + y) * shard, shard), shard)
    own_tokens = pl.ds(pl.multiple_of(c * mine, mine), mine)

    @pl.when(c == 0)
    def _():
        local(value_factor, factor.at[own_rows], 0).start()
        local(saved_in, tokens.at[own_tokens], 1).start()

    @pl.when(c == 1)
    def _():
        local(out_factor, factor.at[own_rows], 0).start()
        local(out_cot, tokens.at[own_tokens], 1).start()

    fetches = [
        local(value_cot, cots.at[0], 2),
        local(mixed_out, cots.at[1], 3),
        local(value_factor, own_factor.at[0], 4),
        local(out_factor, own_factor.at[1], 5),
        local(value_weight, weights.at[0], 6),
        local(out_weight_t, weights.at[1], 7),
        local(value_first, moments.at[0], 8),
        local(value_second, moments.at[1], 9),
        local(out_first, moments.at[2], 10),
        local(out_second, moments.at[3], 11),
    ]
    for fetch in fetches:
        fetch.start()
    pl.semaphore_wait(barrier, len(peers))

    def remote(src, dst, send_sem, recv_sem, to):
        return pltpu.make_async_remote_copy(
            src_ref=src,
            dst_ref=dst,
            send_sem=send_sem,
            recv_sem=recv_sem,
            device_id=to,
            device_id_type=MESH,
        )

    local(value_factor, factor.at[own_rows], 0).wait()

    swap_in = remote(saved_in, tokens.at[own_tokens], tok_sem.at[0], tok_sem.at[1], pair)
    swap_cot = remote(out_cot, tokens.at[own_tokens], tok_sem.at[0], tok_sem.at[1], pair)

    @pl.when(c == 0)
    def _():
        swap_cot.start()

    @pl.when(c == 1)
    def _():
        swap_in.start()

    def order(n):
        shifts = [0]
        for d in range(1, n // 2 + 1):
            shifts.append(-d)
            if d <= (n - 1) // 2:
                shifts.append(d)
        return shifts

    class Color:
        def __init__(self, h):
            self.h = h
            self.na, self.nb = (nz, ny) if h == 0 else (ny, nz)
            self.pa, self.pb = (z, y) if h == 0 else (y, z)
            self.to_a, self.to_b = (at_z, at_y) if h == 0 else (at_y, at_z)
            self.count = 0

        def chunk(self, da, db):
            ia = lax.rem(self.pa + da + self.na, self.na)
            ib = lax.rem(self.pb + db + self.nb, self.nb)
            zi, yi = (ia, ib) if self.h == 0 else (ib, ia)
            return factor.at[shard_rows(zi, yi, self.h)]

        def slot(self, da, db):
            return ga_recv.at[self.h, order(self.na).index(da) * self.nb + order(self.nb).index(db)]

        def send(self, da, db, to, slot):
            ref = self.chunk(da, db)
            remote(ref, ref, ga_send.at[self.h], slot, to).start()
            self.count += 1

        def wait(self, da, db):
            ref = self.chunk(da, db)
            remote(ref, ref, ga_send.at[self.h], self.slot(da, db), pair).wait_recv()

        def on_a(self, da):
            ups, downs = self.na // 2, (self.na - 1) // 2
            if da <= 0 and -da < ups:
                self.send(da, 0, self.to_a(1), self.slot(da - 1, 0))
            if da >= 0 and da < downs:
                self.send(da, 0, self.to_a(-1), self.slot(da + 1, 0))

        def on_b(self, da, db):
            ups, downs = self.nb // 2, (self.nb - 1) // 2
            if db <= 0 and -db < ups:
                self.send(da, db, self.to_b(1), self.slot(da, db - 1))
            if db >= 0 and db < downs:
                self.send(da, db, self.to_b(-1), self.slot(da, db + 1))

        def round(self, t):
            for da in order(self.na):
                if abs(da) == t:
                    if da != 0:
                        self.wait(da, 0)
                    self.on_a(da)
                    self.on_b(da, 0)
            for da in order(self.na):
                for db in order(self.nb):
                    if db != 0 and abs(da) + abs(db) == t:
                        self.wait(da, db)
                        self.on_b(da, db)

        def finish(self):
            ref = factor.at[pl.ds(0, self.count * half)]
            remote(ref, ref, ga_send.at[self.h], ga_recv.at[self.h, 0], pair).wait_send()

    colors = [Color(0), Color(1)]
    for t in range(nz // 2 + ny // 2 + 1):
        for color in colors:
            color.round(t)

    local(saved_in, tokens.at[own_tokens], 1).wait()
    swap_in.wait()

    width = min(512, factor.shape[0])
    acc[...] = jnp.zeros_like(acc)

    @pl.loop(0, factor.shape[0] // width)
    def _(k):
        at = pl.ds(pl.multiple_of(k * width, width), width)
        acc[...] += jnp.dot(tokens[:, at], factor[at, :], preferred_element_type=jnp.float32)

    proj[c] = acc[...].astype(jnp.bfloat16)
    swap_proj = remote(proj.at[c], proj.at[c], proj_sem.at[0], proj_sem.at[1], pair)
    swap_proj.start()
    for fetch in fetches:
        fetch.wait()

    cut = min(256, chans)

    def contract(which):
        left = proj[which]

        @pl.loop(0, chans // cut)
        def _(k):
            at = pl.ds(pl.multiple_of(k * cut, cut), cut)
            part = lax.dot_general(
                left,
                cots[which, :, at],
                (((0,), (0,)), ((), ())),
                preferred_element_type=jnp.float32,
            )
            grads[which, :, :, :, at] = part.reshape(nz, ny, 8, cut)

    contract(c)
    swap_proj.wait_recv()
    contract(1 - c)
    sent = [swap_proj]

    piece = chans // SUBS

    def of_dest(h, dest, sub):
        cols = pl.ds(sub * piece, piece)
        if h == 0:
            return grads[0, :, dest, :, cols].reshape(nz * 8, piece)
        return grads[1, dest, :, :, cols].reshape(ny * 8, piece)

    ring = [(ny, y, at_y, nz, z, at_z), (nz, z, at_z, ny, y, at_y)]

    def step_1(h, step, sub):
        n, pos, to, _, _, _ = ring[h]
        ups, downs = n // 2, (n - 1) // 2
        for way, hops, sign in ((0, ups, 1), (1, downs, -1)):
            if step >= hops:
                continue
            dest = lax.rem(pos + sign * (hops - step) + n, n)
            part = of_dest(h, dest, sub)
            if step > 0:
                wait_1(h, way, step - 1, sub)
                part = part + recv_1[h, way, step - 1, sub].astype(jnp.float32)
            send_1[h, way, step, sub] = part.astype(jnp.bfloat16)
            copy = remote(
                send_1.at[h, way, step, sub],
                recv_1.at[h, way, step, sub],
                s1_send.at[h, way, step, sub],
                s1_recv.at[h, way, step, sub],
                to(sign),
            )
            copy.start()
            sent.append(copy)

    def wait_1(h, way, step, sub):
        remote(
            send_1.at[h, way, step, sub],
            recv_1.at[h, way, step, sub],
            s1_send.at[h, way, step, sub],
            s1_recv.at[h, way, step, sub],
            pair,
        ).wait_recv()

    for step in range(max(nz, ny) // 2):
        for sub in range(SUBS):
            for h in range(2):
                step_1(h, step, sub)

    waits_2 = []
    for h in range(2):
        n, pos, _, m, other, to = ring[h]
        for sub in range(SUBS):
            part = of_dest(h, pos, sub)
            for way, hops in ((0, n // 2), (1, (n - 1) // 2)):
                if hops > 0:
                    wait_1(h, way, hops - 1, sub)
                    part = part + recv_1[h, way, hops - 1, sub].astype(jnp.float32)
            cols = pl.ds(sub * piece, piece)
            part = part.reshape(m, 8, piece)
            own_2[h, :, :, cols] = part
            send_2[h, :, :, cols] = part.astype(jnp.bfloat16)
        for d in range(1, m):
            copy = remote(
                send_2.at[h, lax.rem(other + d, m)],
                recv_2.at[h, d],
                s2_send.at[h, d],
                s2_recv.at[h, d],
                to(d),
            )
            copy.start()
            sent.append(copy)
            waits_2.append(copy)
    for copy in waits_2:
        copy.wait_recv()
    for h in range(2):
        _, _, _, m, other, _ = ring[h]
        part = own_2[h, other]
        for d in range(1, m):
            part = part + recv_2[h, d].astype(jnp.float32)
        recv_3[x, h] = part.astype(jnp.bfloat16)

    waits_3 = []
    for d in range(1, nx):
        copy = remote(recv_3.at[x], recv_3.at[x], s3_send.at[d], s3_recv.at[d], at_x(d))
        copy.start()
        sent.append(copy)
        waits_3.append(copy)
    for copy in waits_3:
        copy.wait_recv()

    for h, (first_new, second_new) in enumerate(((vf_new, vs_new), (of_new, os_new))):
        grad = recv_3[0, h].astype(jnp.float32)
        for k in range(1, nx):
            grad = grad + recv_3[k, h].astype(jnp.float32)
        new_first = beta_first * moments[2 * h] + (1.0 - beta_first) * grad
        new_second = beta_second * moments[2 * h + 1] + (1.0 - beta_second) * grad * grad
        first_new[...] = new_first
        second_new[...] = new_second
        low[h] = (new_first / jnp.sqrt(new_second)).astype(jnp.bfloat16)

    for h in range(2):
        rows_low[h, z, y] = low[h, :, pl.ds(pl.multiple_of(x * quarter, quarter), quarter)]

    waits = []
    for h in range(2):
        n, _, _, m, _, to = ring[h]
        for d in range(1, m):
            ref = rows_low.at[h, z, y]
            copy = remote(ref, ref, e1_send.at[h, d], e1_recv.at[h, d], to(d))
            copy.start()
            sent.append(copy)
            waits.append(copy)
    for copy in waits:
        copy.wait_recv()
    waits = []
    for h in range(2):
        n, _, to, _, _, _ = ring[h]
        for d in range(1, n):
            ref = rows_low.at[0, :, y] if h == 0 else rows_low.at[1, z]
            copy = remote(ref, ref, e2_send.at[h, d], e2_recv.at[h, d], to(d))
            copy.start()
            sent.append(copy)
            waits.append(copy)
    for copy in waits:
        copy.wait_recv()

    square = jnp.zeros((), jnp.float32)
    for h in range(2):
        whole = rows_low[h].reshape(nz * ny * 8, quarter)
        wide = whole.astype(jnp.float32)
        square = square + jnp.sum(wide * wide)
        product[x, h] = jnp.dot(
            own_factor[h], whole, preferred_element_type=jnp.float32
        ).astype(jnp.bfloat16)
    squares[x, c] = jnp.full(squares.shape[2:], square, jnp.float32)

    waits = []
    for k in range(2):
        for d in range(nx):
            if (d, k) == (0, 0):
                continue
            ref = squares.at[x, c]
            copy = remote(
                ref, ref, ss_send.at[k * nx + d], ss_recv.at[k * nx + d], at_x(d, k)
            )
            copy.start()
            sent.append(copy)
            waits.append(copy)
    for d in range(1, nx):
        copy = remote(product.at[x], product.at[x], xp_send.at[d], xp_recv.at[d], at_x(d))
        copy.start()
        sent.append(copy)
        waits.append(copy)
    for copy in waits:
        copy.wait_recv()

    total = squares[0, 0] + squares[0, 1]
    for k in range(1, nx):
        total = total + squares[k, 0] + squares[k, 1]
    spread = jnp.sqrt(total / total_count)
    scale = (clip_level / jnp.maximum(spread, clip_level))[0:1, 0:1]
    for h, (new, copied, step) in enumerate(
        ((vw_new, vw_copy, v_step), (ow_new, ow_copy, o_step))
    ):
        for k in range(nx):
            cols = pl.ds(k * quarter, quarter)
            fresh = weights[h, :, cols] - step_rate * scale * product[k, h].astype(jnp.float32)
            new[:, cols] = fresh
            copied[:, cols] = fresh.astype(jnp.bfloat16)
        step[...] = scale * low[h].astype(jnp.float32)

    for copy in sent:
        copy.wait_send()
    for color in colors:
        color.finish()


def fused(sizes, args):
    nz, ny, nx = sizes
    (saved_in, _, value_cot, _, value_factor, _, value_weight, _, value_first, _, _, _) = args
    shard, rank = value_factor.shape
    model = shard * nz * ny
    mine = saved_in.shape[0]
    chans = value_cot.shape[1]
    quarter = chans // nx
    f32, bf16 = jnp.float32, jnp.bfloat16
    big = max(nz, ny)
    steps = big // 2
    dma = pltpu.SemaphoreType.DMA
    weight = jax.ShapeDtypeStruct(value_weight.shape, f32)
    copied = jax.ShapeDtypeStruct(value_weight.shape, bf16)
    moment = jax.ShapeDtypeStruct(value_first.shape, f32)
    assert nz == ny

    def kernel(*refs):
        body(sizes, 2.0 * rank * 2 * chans, *refs)

    return pl.pallas_call(
        kernel,
        name="update",
        out_shape=(weight, copied, weight, copied) + (moment,) * 6,
        in_specs=[pl.BlockSpec(memory_space=pl.ANY)] * 12,
        out_specs=[pl.BlockSpec(memory_space=pltpu.VMEM)] * 10,
        scratch_shapes=[
            pltpu.VMEM((model, rank), bf16),
            pltpu.VMEM((2 * mine, model), bf16),
            pltpu.VMEM((2 * mine, rank), f32),
            pltpu.VMEM((2, 2 * mine, chans), bf16),
            pltpu.VMEM((2, 2 * mine, rank), bf16),
            pltpu.VMEM((2, nz, ny, 8, chans), f32),
            pltpu.VMEM((2, shard, rank), bf16),
            pltpu.VMEM((2, shard, chans), f32),
            pltpu.VMEM((4, 8, chans), f32),
            pltpu.VMEM((2, 2, steps, SUBS, big * 8, chans // SUBS), bf16),
            pltpu.VMEM((2, 2, steps, SUBS, big * 8, chans // SUBS), bf16),
            pltpu.VMEM((2, big, 8, chans), bf16),
            pltpu.VMEM((2, big, 8, chans), f32),
            pltpu.VMEM((2, big, 8, chans), bf16),
            pltpu.VMEM((nx, 2, 8, chans), bf16),
            pltpu.VMEM((2, 8, chans), bf16),
            pltpu.VMEM((2, nz, ny, 8, quarter), bf16),
            pltpu.VMEM((nx, 2, shard, quarter), bf16),
            pltpu.VMEM((nx, 2, 8, 128), f32),
            dma((12,)),
            dma((2,)),
            dma((2,)),
            dma((2, nz * ny)),
            dma((2,)),
            dma((2, 2, steps, SUBS)),
            dma((2, 2, steps, SUBS)),
            dma((2, big)),
            dma((2, big)),
            dma((nx,)),
            dma((nx,)),
            dma((2, big)),
            dma((2, big)),
            dma((2, big)),
            dma((2, big)),
            dma((nx,)),
            dma((nx,)),
            dma((2 * nx,)),
            dma((2 * nx,)),
        ],
        compiler_params=pltpu.CompilerParams(
            collective_id=0, has_side_effects=True, vmem_limit_bytes=56 * 2**20
        ),
    )(*args)


def solution(mesh):
    side = {256: 16, 64: 8, 16: 4, 4: 2}[mesh.shape["fs"]]
    sizes = (side, side, mesh.shape["rep"])
    torus = Mesh(
        mesh.devices.reshape(side, side, mesh.shape["rep"], mesh.shape["tp"]),
        ("fs_0", "fs_1", "rep", "tp"),
    )

    def shards(*args):
        args = list(args)
        args[7] = args[7].T
        outs = list(fused(sizes, args))
        outs[2], outs[3] = outs[2].T, outs[3].T
        return tuple(outs)

    placed = (
        P(FS_REP_TP, None),
        P(FS_REP_TP, None),
        P(FS_REP, "tp"),
        P(FS_REP, "tp"),
        P(FS, None),
        P(FS, None),
        P(FS, "tp"),
        P("tp", FS),
        P(FS, "tp"),
        P(FS, "tp"),
        P(FS, "tp"),
        P(FS, "tp"),
    )
    return jax.shard_map(
        shards,
        mesh=torus,
        in_specs=placed,
        out_specs=(P(FS, "tp"), P(FS, "tp"), P("tp", FS), P("tp", FS)) + (P(FS, "tp"),) * 6,
        check_vma=False,
    )
```

time: 316 us -> 114 us (0.36)
  waiting for transfers between devices: 200 us -> 0 us
  Pallas kernels: 0 us -> 103 us
  blocking collectives: 82.6 us -> 0 us
  between operations: 14.7 us -> 0.68 us
  matrix products: 10 us -> 0 us
  local copies, waits for them, and re-layouts: 1.8 us -> 8.92 us
  other arithmetic: 6.91 us -> 0 us
    all_gather x2 -> x0, waiting for transfers between devices: 107 us -> none  [the longest x1 107 us: sent_together(): result, at, outs = (lax.all_gather(both, axis, axis=dim, tiled=True), 0, [])]
    pallas_call x0 -> x1, Pallas kernels: none -> 103 us  [fused(): pl.pallas_call(kernel, name='update', out_shape=(weight, copied, weight,...]
    reduce_scatter x2 -> x0, waiting for transfers between devices: 92.7 us -> none  [own_rows(): so_far = lax.psum_scatter(so_far, axis, scatter_dimension=0, tiled=True)]
    psum x3 -> x0, blocking collectives: 48.7 us -> none  [over_axes(): return functools.reduce(lax.psum, axes, array)]
    all_gather x2 -> x0, blocking collectives: 25.4 us -> none  [the longest x1 22.6 us: stacked_from(): blocks = lax.all_gather(blocks, axes[k])]
    dot_general x6 -> x0, matrix products: 10 us -> none  [the longest x1 3.56 us: fold_pair(): jnp.dot(left_in, pieces[0], preferred_element_type=jnp.float32)]
    unnamed x24 -> x28, local copies, waits for them, and re-layouts: 0.07 us -> 8.92 us
    all_to_all x1 -> x0, blocking collectives: 8.54 us -> none  [from_everyone(): lax.all_to_all(jnp.broadcast_to(array[None], (peers, *array.shape)), axis...]
  transfers between devices with their start and end apart: 4 -> 0, of which waited for: 3 -> 0; matrix products, arithmetic and copies ran while one was open for 0% -> 0% of each run, Pallas kernels for 0% -> 0%
where the time goes in v1:
time: 114 us; the launch traced here: 113 us
  Pallas kernels  103 us (90%)
  local copies, waits for them, and re-layouts  8.92 us (8%)
    pallas_call x1, Pallas kernels, fused(): pl.pallas_call(kernel, name='update', out_shape=(weight, copied, weight,...  103 us
    unnamed x28, local copies, waits for them, and re-layouts  8.92 us

profile of v1, /device:TPU:1, one launch (start us, length us, event | category | flops | bytes accessed | tf_op | source)
XLA Modules:
  0.0 112.9 jit_solution(11865100292076090108)
XLA Ops:
  0.6 103.3 %update.1 = (f32[64,1024]{1,0:T(8,128)}, bf16[64,1024]{1,0:T(8,128)(2,1)}, f32[64,1024]{1,0:T(8,128)}, bf16[64,1024]{1,0:T(8,128)(2,1)}, f32[8,1024]{1,0:T(8,128...) custom-call(bf16[128,4096]{1,0:T(8,128)(2,1)} %refs_0_.1, ...), custom_call_target="tpu_custom_call" | custom-call | tf_op jit(solution)/shard_map/update/pallas_call | solution.py:473
  104.0 0.0 copy-start.2
  104.0 1.7 %copy.32 = f32[64,1024]{1,0:T(8,128)} copy(f32[64,1024]{1,0:T(8,128)} %get-tuple-element.40) | data formatting | bytes 524288
  105.7 0.0 copy-done.2
  105.7 0.0 copy-start
  105.7 0.7 copy.33
  106.4 0.3 copy-done
  106.7 0.0 copy-start.1
  106.7 0.7 copy.34
  107.4 0.3 copy-done.1
  107.7 0.0 copy-start.8
  107.7 0.7 copy.35
  108.4 0.1 copy-done.8
  108.5 0.0 copy-start.7
  108.5 0.6 copy.36
  109.1 0.2 copy-done.7
  109.2 0.0 copy-start.6
  109.2 0.6 copy.37
  109.9 0.2 copy-done.6
  110.0 0.0 copy-start.5
  110.0 0.6 copy.38
  110.6 0.2 copy-done.5
  110.8 0.0 copy-start.4
  110.8 0.6 copy.39
  111.4 0.2 copy-done.4
  111.6 0.0 copy-start.3
  111.6 0.6 copy.40
  112.2 0.2 copy-done.3
  112.3 0.6 copy.41
Async XLA Ops:
  104.0 1.7 %copy-start.2 = (bf16[64,1024]{1,0:T(8,128)(2,1)S(1)}, bf16[64,1024]{1,0:T(8,128)(2,1)}, u32[]{:S(2)}) copy-start(bf16[64,1024]{1,0:T(8,128)(2,1)} %get-tuple-element.41) | copy-start | bytes 393220
  105.7 1.0 copy-start
  106.7 1.0 copy-start.1
  107.7 0.8 copy-start.8
  108.5 0.8 copy-start.7
  109.2 0.8 copy-start.6
  110.0 0.8 copy-start.5
  110.8 0.8 copy-start.4
  111.6 0.8 copy-start.3
